TPU v7x, 32 devices: a whole 2x2x4 slice. The times are simulated.
32 devices in a mesh: sp: 16 (over z, y, x), tp: 2 (over core).
Axes of the slice: x: 2, y: 2, z: 4, core: 2. Of those that a mesh axis runs over, the one named last changes fastest.
Arguments:
- proj_a: bfloat16 [4096, 3072], P('sp', 'tp'), may hold values from -20 to 20
- proj_gate: bfloat16 [4096, 3072], P('sp', 'tp'), may hold values from -6 to 6
- taps: bfloat16 [31, 3072], P(None, 'tp'), may hold values from -1 to 1
- norm_gain: float32 [3072], P('tp'), may hold values from 0.1 to 1.9
- norm_shift: float32 [3072], P('tp'), may hold values from -3 to 3
- cotangent: bfloat16 [4096, 3072], P('sp', 'tp'), may hold values from -6 to 6
Outputs:
- a_grad: bfloat16 [4096, 3072], P('sp', 'tp')
- gate_grad: bfloat16 [4096, 3072], P('sp', 'tp')
- taps_grad: float32 [31, 3072], P(None, 'tp')
- gain_grad: float32 [3072], P('tp')
- shift_grad: float32 [3072], P('tp')
All inputs are finite; a program needn't handle non-finite values.
Results may differ from a plain program's by a relative error of at most 0.0048.
Values may be sent and summed in bfloat16 or wider, within the bound.
A program may use at most 64 MiB of HBM per device.

v0:
```python
import jax
import jax.numpy as jnp
from jax import lax
from jax.sharding import PartitionSpec as P

D = 3072


EPS = 1e-05


def from_behind(x, axis, by):
    size = lax.axis_size(axis)
    pairs = [(i, i + by) for i in range(size) if 0 <= i + by < size]
    return lax.ppermute(x, axis, pairs)


def gated(a_rows, g_rows):
    return (a_rows.astype(jnp.float32) * jax.nn.sigmoid(g_rows.astype(jnp.float32))).astype(
        jnp.bfloat16
    )


def depthwise(source, tapf, count):
    total = jnp.zeros((count, source.shape[1]), jnp.float32)
    for k in range(tapf.shape[0]):
        total = total + tapf[k] * source[k : k + count].astype(jnp.float32)
    return total


def transposed(source, tapf, count):
    edge = tapf.shape[0] - 1
    total = jnp.zeros((count, source.shape[1]), jnp.float32)
    for k in range(tapf.shape[0]):
        total = total + tapf[edge - k] * source[k : k + count]
    return total


def norm_backward(conv, cot_rows, gain, shift):
    first_sum, second_sum = lax.psum(
        (jnp.sum(conv, axis=1, keepdims=True), jnp.sum(conv * conv, axis=1, keepdims=True)), "tp"
    )
    mean = first_sum / D
    cent = conv - mean
    spread = jnp.maximum(second_sum / D - mean * mean, 0.0)
    rstd = lax.rsqrt(spread + EPS)
    normed = cent * rstd
    pre = normed * gain + shift
    sig = jax.nn.sigmoid(pre)
    dpre = cot_rows.astype(jnp.float32) * sig * (1.0 + pre * (1.0 - sig))
    dnormed = dpre * gain
    dn_sum, dn_dot = lax.psum(
        (jnp.sum(dnormed, axis=1, keepdims=True), jnp.sum(dnormed * normed, axis=1, keepdims=True)),
        "tp",
    )
    dconv = rstd * (dnormed - dn_sum / D - normed * (dn_dot / D))
    return (dconv, dpre, normed)


def body(proj_a, proj_gate, taps, norm_gain, norm_shift, cotangent):
    width = taps.shape[0]
    edge = width - 1
    rows = proj_a.shape[0]
    chans = proj_a.shape[1]
    tapf = taps.astype(jnp.float32)
    glu = gated(proj_a, proj_gate)
    before = from_behind(glu[rows - edge :], "sp", 1)
    glu_all = jnp.concatenate([before, glu], axis=0)
    conv = depthwise(glu_all, tapf, rows)
    dconv, dpre, normed = norm_backward(conv, cotangent, norm_gain, norm_shift)
    pad = jnp.zeros((edge, chans), jnp.float32)
    spread_rows = transposed(jnp.concatenate([pad, dconv, pad], axis=0), tapf, rows + edge)
    returned = from_behind(spread_rows[:edge], "sp", -1)
    mine = spread_rows[edge:]
    dglu = jnp.concatenate([mine[: rows - edge], mine[rows - edge :] + returned], axis=0)
    taps_part = jnp.stack(
        [jnp.sum(dconv * glu_all[j : j + rows].astype(jnp.float32), axis=0) for j in range(width)]
    )
    gain_part = jnp.sum(dpre * normed, axis=0)
    shift_part = jnp.sum(dpre, axis=0)
    taps_grad, gain_grad, shift_grad = lax.psum((taps_part, gain_part, shift_part), "sp")
    sg = jax.nn.sigmoid(proj_gate.astype(jnp.float32))
    a_grad = (dglu * sg).astype(jnp.bfloat16)
    gate_grad = (dglu * proj_a.astype(jnp.float32) * sg * (1.0 - sg)).astype(jnp.bfloat16)
    return (a_grad, gate_grad, taps_grad, gain_grad, shift_grad)


def solution(mesh):
    placed = (P("sp", "tp"), P("sp", "tp"), P(None, "tp"), P("tp"), P("tp"), P("sp", "tp"))
    return jax.shard_map(
        body,
        mesh=mesh,
        in_specs=placed,
        out_specs=(P("sp", "tp"), P("sp", "tp"), P(None, "tp"), P("tp"), P("tp")),
        check_vma=False,
    )
```

profile of v0, /device:TPU:0, one launch (start us, length us, event | category | flops | bytes accessed | tf_op | source)
XLA Modules:
  0.0 185.9 jit_solution(1239141731191796493)
XLA Ops:
  7.2 1.8 fusion.30
  9.1 4.9 %collective-permute-start = (bf16[30,1536]{1,0:T(8,128)(2,1)S(1)}, bf16[30,1536]{1,0:T(8,128)(2,1)S(1)}, u32[]{:S(2)}, u32[]{:S(2)}) collective-permute-start(bf16[30,1536]{1,0:T(8,128)(2,1)S(1)} %slice.446), channel_id=1, source_target_pairs={{0,2},{2,4},{4,6},{6,8},{8,10},{10,12},{12,14},{14,16},{16,18},{18... | collective-permute-start | bytes 276488 | tf_op jit(solution)/shard_map/ppermute | solution.py:15
  14.7 1.4 collective-permute-done
  16.2 8.5 %multiply_reduce_fusion.2 = (f32[256]{0:T(256)S(1)}, f32[256]{0:T(256)S(1)}, f32[256,1536]{1,0:T(8,128)S(1)}) fusion(bf16[256,1536]{1,0:T(8,128)(2,1)S(1)} %fusion.30, f32[1536]{0:T(1024)S(1)} %get-tuple-element.72, bf16[30,1536]{1,0:T(8,128)(2,1)S(1)} %collective-permute-done, f32[1536]{0:T(1024)S(1)} %get-tuple-element.43, ...), kind=kLoop, calls=%fused_computation.225 | loop fusion | flops 72744448 | bytes 2643968 | tf_op jit(solution)/shard_map/reduce_sum | solution.py:41
  24.7 2.5 %all-reduce.4 = (f32[256,1]{0,1:T(1,128)S(1)}, f32[256,1]{0,1:T(1,128)S(1)}) all-reduce(f32[256,1]{0,1:T(1,128)S(1)} %bitcast.15, f32[256,1]{0,1:T(1,128)S(1)} %bitcast.14), channel_id=1, replica_groups=mesh['sp'=16,'tp'=2] {'tp'}, use_global_device_ids=true, to_apply=%region_3.0 | all-reduce | flops 512 | bytes 4096 | tf_op jit(solution)/shard_map/psum | solution.py:40
  27.2 2.9 %multiply_reduce_fusion = (f32[1536]{0:T(1024)}, f32[256]{0:T(256)S(1)}, f32[256]{0:T(256)S(1)}, f32[1536]{0:T(1024)}, f32[256,1536]{1,0:T(8,128)}) fusion(f32[256,1536]{1,0:T(8,128)S(1)} %get-tuple-element.81, f32[256]{0:T(256)S(1)} %bitcast.10, f32[256]{0:T(256)S(1)} %bitcast.8, f32[1536]{0:T(1024)S(1)} %copy-done.36, f32[1536]{0:T(1024)S(1)} %copy-done.39, ...), kind=kLoop, calls=%fused_computation.219 | loop fusion | flops 7860736 | bytes 3960832 | tf_op jit(solution)/shard_map/reduce_sum | solution.py:79
  30.3 2.5 %all-reduce.3 = (f32[256,1]{0,1:T(1,128)S(1)}, f32[256,1]{0,1:T(1,128)S(1)}) all-reduce(f32[256,1]{0,1:T(1,128)S(1)} %bitcast.12, f32[256,1]{0,1:T(1,128)S(1)} %bitcast.13), channel_id=1, replica_groups=mesh['sp'=16,'tp'=2] {'tp'}, use_global_device_ids=true, to_apply=%region_7.0 | all-reduce | flops 512 | bytes 4096 | tf_op jit(solution)/shard_map/psum | solution.py:52
  32.8 3.4 %fusion.93 = (f32[1536]{0:T(1024)S(1)}, f32[1536]{0:T(1024)S(1)}, f32[1536]{0:T(1024)S(1)}, f32[1536]{0:T(1024)S(1)}, f32[1536]{0:T(1024)S(1)}, /*index=5*/f32[1...) fusion(bf16[256,1536]{1,0:T(8,128)(2,1)S(1)} %fusion.30, bf16[30,1536]{1,0:T(8,128)(2,1)S(1)} %collective-permute-done, ...), kind=kLoop, calls=%fused_computation.216 | loop fusion | flops 18077184 | bytes 5650432 | tf_op jit(solution)/shard_map/reduce_sum | solution.py:77
  37.1 6.7 %fusion.1 = f32[286,1536]{1,0:T(8,128)S(1)} fusion(f32[316,1536]{1,0:T(8,128)S(1)} %pad_maximum_fusion, f32[256,1536]{1,0:T(8,128)S(1)} %get-tuple-element.79, f32[1536]{0:T(1024)S(1)} %get-tuple-element.42, f32[1536]{0:T(1024)S(1)} %copy-done.13, f32[1536]{0:T(1024)S(1)} %copy-done.33, f32[1536]{0:T(1024)S(1)} %copy-done.31, f32[1536]{0:T(1024)S(1)} %copy-done.29, ...), kind=kLoop, calls=%fused_computation.96 | loop fusion | flops 26797056 | bytes 54478848 | tf_op jit(solution)/shard_map/add | solution.py:35
  43.9 1.3 collective-permute-start.1
  45.2 1.4 fusion.64
  46.6 1.4 fusion.70
  48.0 1.4 fusion.76
  49.4 1.4 fusion.82
  51.1 0.6 stack.112
  51.7 0.6 stack.113
  52.3 0.6 stack.114
  52.9 0.6 stack.115
  53.5 0.6 stack.116
  54.1 0.6 stack.117
  54.7 0.6 stack.118
  55.3 0.6 stack.119
  55.9 0.6 stack.96
  56.5 0.6 stack.97
  57.7 0.6 stack.99
  58.9 0.6 stack.121
  59.6 5.0 %stack.127 = f32[31,1536]{1,0:T(8,128)} concatenate(f32[1,1536]{1,0:T(1,128)} %stack.96, f32[1,1536]{1,0:T(1,128)} %stack.97, f32[1,1536]{1,0:T(1,128)} %stack.98, f32[1,1536]{1,0:T(1,128)} %stack.99, f32[1,1536]{1,0:T(1,128)S(1)} %stack.100, f32[1,1536]{1,0:T(1,128)S(1)} %stack.101, f32[1,1536]{1,0:T(1,128)S(1)} %stack.102, f32[1,1536]{1,0:T(1,128)S(1)} %stack.103, ...), dimensions={0} | concatenate | bytes 380928 | tf_op jit(solution)/shard_map/stack | solution.py:76
  64.6 80.8 %all-reduce.2 = (f32[1536]{0:T(1024)}, f32[1536]{0:T(1024)}) all-reduce(f32[1536]{0:T(1024)S(1)} %copy-done.37, f32[1536]{0:T(1024)S(1)} %copy-done.38), channel_id=1, replica_groups=mesh['sp'=16,'tp'=2] {'sp'}, use_global_device_ids=true, to_apply=%region_41.0 | all-reduce | flops 3072 | bytes 24576 | tf_op jit(solution)/shard_map/psum | solution.py:81
  145.4 1.0 slice_add_fusion
  146.4 3.2 %fusion.33 = (bf16[256,1536]{1,0:T(8,128)(2,1)}, bf16[256,1536]{1,0:T(8,128)(2,1)}) fusion(bf16[256,1536]{1,0:T(8,128)(2,1)} %param.6, f32[30,1536]{1,0:T(8,128)S(1)} %slice_add_fusion, f32[226,1536]{1,0:T(8,128)S(1)} %slice.563, bf16[256,1536]{1,0:T(8,128)(2,1)} %param.7), kind=kLoop, calls=%fused_computation.156 | loop fusion | flops 5111808 | bytes 4718592 | tf_op jit(solution)/shard_map/convert_element_type | solution.py:84
  149.5 27.9 %all-reduce.7.cloned.1.call-done = f32[31,1536]{1,0:T(8,128)} async-done(((f32[31,1536]{1,0:T(8,128)}), f32[31,1536]{1,0:T(8,128)}) %all-reduce.7.cloned.1.call-update) | async-done | bytes 190480 | tf_op jit(solution)/shard_map/psum | solution.py:81
  177.4 1.6 copy.12
  (112 shorter events, 3.0 us)
Async XLA Ops:
  7.2 6.8 %copy-start.1 = (bf16[31,1536]{1,0:T(8,128)(2,1)S(1)}, bf16[31,1536]{1,0:T(8,128)(2,1)}, u32[]{:S(2)}) copy-start(bf16[31,1536]{1,0:T(8,128)(2,1)} %param.8) | copy-start | bytes 285700
  7.2 170.2 %all-reduce.7.cloned.1.call-start = ((), (), s32[]{:S(2)}) async-start(), calls=%async_computation | async-start | bytes 393216 | tf_op jit(solution)/shard_map/psum | solution.py:81
  9.1 7.1 %collective-permute-start = (bf16[30,1536]{1,0:T(8,128)(2,1)S(1)}, bf16[30,1536]{1,0:T(8,128)(2,1)S(1)}, u32[]{:S(2)}, u32[]{:S(2)}) collective-permute-start(bf16[30,1536]{1,0:T(8,128)(2,1)S(1)} %slice.446), channel_id=1, source_target_pairs={{0,2},{2,4},{4,6},{6,8},{8,10},{10,12},{12,14},{14,16},{16,18},{18... | collective-permute-start | bytes 276488 | tf_op jit(solution)/shard_map/ppermute | solution.py:15
  14.0 13.2 %copy-start = (bf16[256,1536]{1,0:T(8,128)(2,1)S(1)}, bf16[256,1536]{1,0:T(8,128)(2,1)}, u32[]{:S(2)}) copy-start(bf16[256,1536]{1,0:T(8,128)(2,1)} %param.11) | copy-start | bytes 2359300
  14.0 13.2 %copy-start.36 = (f32[1536]{0:T(1024)S(1)}, f32[1536]{0:T(1024)}, u32[]{:S(2)}) copy-start(f32[1536]{0:T(1024)} %param.9) | copy-start | bytes 18436
  14.0 13.2 %copy-start.39 = (f32[1536]{0:T(1024)S(1)}, f32[1536]{0:T(1024)}, u32[]{:S(2)}) copy-start(f32[1536]{0:T(1024)} %param.10) | copy-start | bytes 18436
  14.4 15.8 %copy-start.2 = (f32[1536]{0:T(1024)}, f32[1536]{0:T(1024)S(1)}, u32[]{:S(2)}) copy-start(f32[1536]{0:T(1024)S(1)} %get-tuple-element.56) | copy-start | bytes 18436
  14.4 15.8 %copy-start.4 = (f32[1536]{0:T(1024)}, f32[1536]{0:T(1024)S(1)}, u32[]{:S(2)}) copy-start(f32[1536]{0:T(1024)S(1)} %get-tuple-element.57) | copy-start | bytes 18436
  14.4 15.8 %copy-start.6 = (f32[1536]{0:T(1024)}, f32[1536]{0:T(1024)S(1)}, u32[]{:S(2)}) copy-start(f32[1536]{0:T(1024)S(1)} %get-tuple-element.58) | copy-start | bytes 18436
  14.4 15.8 %copy-start.8 = (f32[1536]{0:T(1024)}, f32[1536]{0:T(1024)S(1)}, u32[]{:S(2)}) copy-start(f32[1536]{0:T(1024)S(1)} %get-tuple-element.59) | copy-start | bytes 18436
  14.4 15.8 %copy-start.10 = (f32[1536]{0:T(1024)}, f32[1536]{0:T(1024)S(1)}, u32[]{:S(2)}) copy-start(f32[1536]{0:T(1024)S(1)} %get-tuple-element.60) | copy-start | bytes 18436
  14.6 15.6 %copy-start.12 = (f32[1536]{0:T(1024)}, f32[1536]{0:T(1024)S(1)}, u32[]{:S(2)}) copy-start(f32[1536]{0:T(1024)S(1)} %get-tuple-element.61) | copy-start | bytes 18436
  14.6 15.6 %copy-start.14 = (f32[1536]{0:T(1024)}, f32[1536]{0:T(1024)S(1)}, u32[]{:S(2)}) copy-start(f32[1536]{0:T(1024)S(1)} %get-tuple-element.62) | copy-start | bytes 18436
  14.6 15.6 %copy-start.16 = (f32[1536]{0:T(1024)}, f32[1536]{0:T(1024)S(1)}, u32[]{:S(2)}) copy-start(f32[1536]{0:T(1024)S(1)} %get-tuple-element.63) | copy-start | bytes 18436
  14.6 15.6 %copy-start.18 = (f32[1536]{0:T(1024)}, f32[1536]{0:T(1024)S(1)}, u32[]{:S(2)}) copy-start(f32[1536]{0:T(1024)S(1)} %get-tuple-element.64) | copy-start | bytes 18436
  14.6 15.6 %copy-start.20 = (f32[1536]{0:T(1024)}, f32[1536]{0:T(1024)S(1)}, u32[]{:S(2)}) copy-start(f32[1536]{0:T(1024)S(1)} %get-tuple-element.65) | copy-start | bytes 18436
  14.7 15.6 %copy-start.22 = (f32[1536]{0:T(1024)}, f32[1536]{0:T(1024)S(1)}, u32[]{:S(2)}) copy-start(f32[1536]{0:T(1024)S(1)} %get-tuple-element.66) | copy-start | bytes 18436
  14.7 15.6 %copy-start.24 = (f32[1536]{0:T(1024)}, f32[1536]{0:T(1024)S(1)}, u32[]{:S(2)}) copy-start(f32[1536]{0:T(1024)S(1)} %get-tuple-element.67) | copy-start | bytes 18436
  14.7 15.6 %copy-start.26 = (f32[1536]{0:T(1024)}, f32[1536]{0:T(1024)S(1)}, u32[]{:S(2)}) copy-start(f32[1536]{0:T(1024)S(1)} %get-tuple-element.68) | copy-start | bytes 18436
  14.7 15.6 %copy-start.28 = (f32[1536]{0:T(1024)}, f32[1536]{0:T(1024)S(1)}, u32[]{:S(2)}) copy-start(f32[1536]{0:T(1024)S(1)} %get-tuple-element.69) | copy-start | bytes 18436
  14.7 15.6 %copy-start.30 = (f32[1536]{0:T(1024)}, f32[1536]{0:T(1024)S(1)}, u32[]{:S(2)}) copy-start(f32[1536]{0:T(1024)S(1)} %get-tuple-element.70) | copy-start | bytes 18436
  14.7 15.6 %copy-start.32 = (f32[1536]{0:T(1024)}, f32[1536]{0:T(1024)S(1)}, u32[]{:S(2)}) copy-start(f32[1536]{0:T(1024)S(1)} %get-tuple-element.71) | copy-start | bytes 18436
  14.7 15.6 %copy-start.34 = (f32[1536]{0:T(1024)}, f32[1536]{0:T(1024)S(1)}, u32[]{:S(2)}) copy-start(f32[1536]{0:T(1024)S(1)} %get-tuple-element.72) | copy-start | bytes 18436
  36.3 0.8 copy-start.25
  36.3 0.8 copy-start.27
  36.3 0.8 copy-start.29
  36.3 0.8 copy-start.31
  36.3 0.8 copy-start.33
  36.3 0.8 copy-start.35
  43.9 101.5 %collective-permute-start.1 = (f32[30,1536]{1,0:T(8,128)S(1)}, f32[30,1536]{1,0:T(8,128)}, u32[]{:S(2)}, u32[]{:S(2)}) collective-permute-start(f32[30,1536]{1,0:T(8,128)S(1)} %slice.565), channel_id=1, source_target_pairs={{2,0},{4,2},{6,4},{8,6},{10,8},{12,10},{14,12},{16,14},{18,16},{20... | collective-permute-start | bytes 552968 | tf_op jit(solution)/shard_map/ppermute | solution.py:15
  50.8 13.8 %copy-start.37 = (f32[1536]{0:T(1024)S(1)}, f32[1536]{0:T(1024)}, u32[]{:S(2)}) copy-start(f32[1536]{0:T(1024)} %get-tuple-element.5) | copy-start | bytes 18436
  50.8 13.8 %copy-start.38 = (f32[1536]{0:T(1024)S(1)}, f32[1536]{0:T(1024)}, u32[]{:S(2)}) copy-start(f32[1536]{0:T(1024)} %get-tuple-element.39) | copy-start | bytes 18436
  (11 other events, 8.0 us)
Sparse Core Ops, SparseCore 0:
  64.7 112.6 all-reduce.6
where the time goes:
time: 186 us
  blocking collectives  85.7 us (46%)
  other arithmetic  33.4 us (18%)
  waiting for transfers between devices  29.3 us (16%)
  local copies, waits for them, and re-layouts  16.5 us (9%)
  between operations  14.8 us (8%)
  starting transfers between devices  6.21 us (3%)
    psum x1, blocking collectives, body(): lax.psum((taps_part, gain_part, shift_part), 'sp')  80.8 us
    psum x1, waiting for transfers between devices, body(): lax.psum((taps_part, gain_part, shift_part), 'sp')  27.9 us
    another operation x32, local copies, waits for them, and re-layouts, body(): jnp.stack([jnp.sum(dconv * glu_all[j:j + rows].astype(jnp.float32), axis=...  13.5 us
    reduce_sum x5, other arithmetic, body(): jnp.sum(dconv * glu_all[j:j + rows].astype(jnp.float32), axis=0)  8.97 us
    reduce_sum x1, other arithmetic, norm_backward(): jnp.sum(conv * conv, axis=1, keepdims=True)  8.52 us
    add x1, other arithmetic, transposed(): total = total + tapf[edge - k] * source[k:k + count]  6.72 us
    ppermute x2, starting transfers between devices, from_behind(): return lax.ppermute(x, axis, pairs)  6.17 us
  transfers between devices with their start and end apart: 3, of which 2 were waited for; matrix products, arithmetic and copies ran while one was open for 13% of the time, Pallas kernels for 0%

commit v1 on v0

v1 whole, which is shorter than its diff:
```python
import functools

import jax
import jax.numpy as jnp
from jax import lax
from jax.experimental import pallas as pl
from jax.experimental.pallas import tpu as pltpu
from jax.sharding import PartitionSpec as P

EPS = 1e-05
LANES = 128
SUB = 8
BLOCK = 64
HALO = 32
F32 = jnp.float32
BF16 = jnp.bfloat16


def plan(chans, width, n):
    tiles = chans // LANES
    group = -(-(width + 2) // SUB) * SUB
    units = tiles * (group // SUB)
    per = -(-units // n)
    owners = -(-units // per)
    return tiles, group, per * SUB, owners


def kernel(
    n, ntp, width, full,
    a_ref, g_ref, taps_ref, gain_ref, shift_ref, cot_ref,
    ag_ref, gg_ref, tg_ref, gaing_ref, shiftg_ref,
    x_s, conv_s, dn_s, d_s, taps_s, par_s,
    glu_out, glu_in, dc_out, dc_in,
    st_out, st_in, stat_s,
    red_s, rs_in, ag_src, ag_in,
    halo_send, halo_recv, st_send, st_recv,
    rs_send, rs_recv, ag_send, ag_recv,
):
    rows, chans = a_ref.shape
    edge = width - 1
    lead = HALO - edge
    tiles, group, chunk, owners = plan(chans, width, n)
    blocks = rows // BLOCK
    me = lax.axis_index("sp")
    core = lax.axis_index("tp")
    other = 1 - core

    barrier = pltpu.get_barrier_semaphore()

    def greet(step, carry):
        pl.semaphore_signal(barrier, inc=1, device_id={"sp": lax.rem(me + step, n)})
        return carry

    lax.fori_loop(1, n, greet, 0)
    pl.semaphore_signal(barrier, inc=1, device_id={"tp": other})

    def cols(j):
        return pl.ds(pl.multiple_of(j * LANES, LANES), LANES)

    def gate_tile(j, base, count):
        a = a_ref[pl.ds(base, count), cols(j)].astype(F32)
        g = g_ref[pl.ds(base, count), cols(j)].astype(F32)
        return (a * jax.nn.sigmoid(g)).astype(BF16)

    def last_rows(j, carry):
        glu_out[j] = gate_tile(j, rows - HALO, HALO)
        return carry

    lax.fori_loop(0, tiles, last_rows, 0)
    pl.semaphore_wait(barrier, n)

    glu_copy = pltpu.make_async_remote_copy(
        src_ref=glu_out, dst_ref=glu_in, send_sem=halo_send.at[0], recv_sem=halo_recv.at[0],
        device_id={"sp": lax.rem(me + 1, n)},
    )
    dc_copy = pltpu.make_async_remote_copy(
        src_ref=dc_out, dst_ref=dc_in, send_sem=halo_send.at[1], recv_sem=halo_recv.at[1],
        device_id={"sp": lax.rem(me + n - 1, n)},
    )

    @pl.when(me < n - 1)
    def _():
        glu_copy.start()

    def prepare(j, carry):
        taps_s[j, pl.ds(0, width), :] = taps_ref[:, cols(j)].astype(F32)
        par_s[j, 0:1, :] = gain_ref[:, cols(j)]
        par_s[j, 1:2, :] = shift_ref[:, cols(j)]
        for b in range(blocks):
            x_s[j, pl.ds(HALO + b * BLOCK, BLOCK), :] = gate_tile(j, b * BLOCK, BLOCK).astype(F32)
        return carry

    lax.fori_loop(0, tiles, prepare, 0)

    lane = lax.broadcasted_iota(jnp.int32, (BLOCK, LANES), 1)

    def stat_copy(i):
        return pltpu.make_async_remote_copy(
            src_ref=st_out.at[i], dst_ref=st_in.at[i], send_sem=st_send.at[i],
            recv_sem=st_recv.at[i], device_id={"tp": other},
        )

    def send_stats(i, first, second):
        first = jnp.sum(first, axis=1, keepdims=True)
        second = jnp.sum(second, axis=1, keepdims=True)
        st_out[i] = jnp.where(lane < LANES // 2, first, second)
        stat_copy(i).start()

    def both_stats(i):
        stat_copy(i).wait_recv()
        both = (st_out[i] + st_in[i]) * (1.0 / full)
        first = jnp.broadcast_to(both[:, 0:1], (BLOCK, LANES))
        second = jnp.broadcast_to(both[:, LANES // 2 : LANES // 2 + 1], (BLOCK, LANES))
        return first, second

    zero = jnp.zeros((BLOCK, LANES), F32)

    def convolve(b):
        base = b * BLOCK

        def step(j, carry):
            first, second = carry
            acc = zero
            for k in range(width):
                acc = acc + taps_s[j, k : k + 1, :] * x_s[j, pl.ds(base + lead + k, BLOCK), :]
            conv_s[j, pl.ds(base, BLOCK), :] = acc
            return first + acc, second + acc * acc

        first, second = lax.fori_loop(0, tiles, step, (zero, zero))
        send_stats(b, first, second)

    order = list(range(1, blocks)) + [0]
    for b in order[:-1]:
        convolve(b)

    @pl.when(me > 0)
    def _():
        glu_copy.wait_recv()

        def widen(j, carry):
            x_s[j, pl.ds(0, HALO), :] = glu_in[j].astype(F32)
            return carry

        lax.fori_loop(0, tiles, widen, 0)

    @pl.when(me == 0)
    def _():
        def clear(j, carry):
            x_s[j, pl.ds(0, HALO), :] = jnp.zeros((HALO, LANES), F32)
            return carry

        lax.fori_loop(0, tiles, clear, 0)

    convolve(0)

    def clear_sums(j, carry):
        par_s[j, pl.ds(SUB, 2 * SUB), :] = jnp.zeros((2 * SUB, LANES), F32)
        return carry

    lax.fori_loop(0, tiles, clear_sums, 0)

    def fold(x):
        return jnp.sum(x.reshape(x.shape[0] // SUB, SUB, LANES), axis=0)

    def normalise(b):
        base = b * BLOCK
        mean, square = both_stats(b)
        rstd = lax.rsqrt(jnp.maximum(square - mean * mean, 0.0) + EPS)
        stat_s[0, pl.ds(base, BLOCK), :] = rstd

        def step(j, carry):
            first, second = carry
            at = pl.ds(base, BLOCK)
            gain = par_s[j, 0:1, :]
            normed = (conv_s[j, at, :] - mean) * rstd
            pre = normed * gain + par_s[j, 1:2, :]
            sig = jax.nn.sigmoid(pre)
            dpre = cot_ref[at, cols(j)].astype(F32) * sig * (1.0 + pre * (1.0 - sig))
            par_s[j, pl.ds(SUB, SUB), :] += fold(dpre * normed)
            par_s[j, pl.ds(2 * SUB, SUB), :] += fold(dpre)
            dn = dpre * gain
            conv_s[j, at, :] = normed
            dn_s[j, at, :] = dn
            return first + dn, second + dn * normed

        first, second = lax.fori_loop(0, tiles, step, (zero, zero))
        send_stats(blocks + b, first, second)

    def take_stats(b):
        first, second = both_stats(blocks + b)
        at = pl.ds(b * BLOCK, BLOCK)
        stat_s[1, at, :] = first
        stat_s[2, at, :] = second

    def dconv_at(j, at):
        return stat_s[0, at, :] * (
            dn_s[j, at, :] - stat_s[1, at, :] - conv_s[j, at, :] * stat_s[2, at, :]
        )

    for b in range(blocks):
        normalise(b)
        if b == 1 or blocks == 1:
            take_stats(0)

            def head(j, carry):
                dc_out[j] = dconv_at(j, pl.ds(0, HALO)).astype(BF16)
                return carry

            lax.fori_loop(0, tiles, head, 0)

            @pl.when(me > 0)
            def _():
                dc_copy.start()

    for b in range(1, blocks):
        take_stats(b)

    def taps_step(j, carry):
        def tile(r, accs):
            base = pl.multiple_of(r * 2 * SUB, 2 * SUB)
            d = dconv_at(j, pl.ds(base, 2 * SUB))
            d_s[j, pl.ds(base, 2 * SUB), :] = d
            out = []
            for k in range(width):
                prod = d * x_s[j, pl.ds(base + lead + k, 2 * SUB), :]
                out.append(accs[k] + (prod[:SUB] + prod[SUB:]))
            return tuple(out)

        start = tuple(jnp.zeros((SUB, LANES), F32) for _ in range(width))
        accs = lax.fori_loop(0, rows // (2 * SUB), tile, start)
        at = pl.multiple_of(j * group, SUB)
        for k in range(width):
            red_s[pl.ds(at + k, 1), :] = jnp.sum(accs[k], axis=0, keepdims=True)
        for k in range(2):
            red_s[pl.ds(at + width + k, 1), :] = jnp.sum(
                par_s[j, pl.ds(SUB + k * SUB, SUB), :], axis=0, keepdims=True
            )
        for k in range(width + 2, group):
            red_s[pl.ds(at + k, 1), :] = jnp.zeros((1, LANES), F32)
        return carry

    lax.fori_loop(0, tiles, taps_step, 0)
    spare = owners * chunk - tiles * group
    if spare:
        red_s[pl.ds(tiles * group, spare), :] = jnp.zeros((spare, LANES), F32)

    def part(owner):
        return pl.ds(pl.multiple_of(owner * chunk, SUB), chunk)

    def rs_copy(owner, source, to):
        return pltpu.make_async_remote_copy(
            src_ref=red_s.at[part(owner)], dst_ref=rs_in.at[source],
            send_sem=rs_send.at[owner], recv_sem=rs_recv.at[source], device_id={"sp": to},
        )

    def ag_copy(owner, to):
        return pltpu.make_async_remote_copy(
            src_ref=ag_src, dst_ref=ag_in.at[part(owner)],
            send_sem=ag_send.at[to], recv_sem=ag_recv.at[owner], device_id={"sp": to},
        )

    def peers(run, limit=n):
        def step(d, carry):
            peer = lax.rem(me + d, n)
            if limit == n:
                run(peer)
            else:
                pl.when(peer < limit)(lambda: run(peer))
            return carry

        lax.fori_loop(1, n, step, 0)

    peers(lambda peer: rs_copy(peer, me, peer).start(), owners)

    def back(b):
        base = b * BLOCK

        def step(j, carry):
            acc = zero
            for k in range(width):
                acc = acc + taps_s[j, edge - k : edge - k + 1, :] * d_s[j, pl.ds(base + k, BLOCK), :]
            at = pl.ds(base, BLOCK)
            sg = jax.nn.sigmoid(g_ref[at, cols(j)].astype(F32))
            first = acc * sg
            ag_ref[at, cols(j)] = first.astype(BF16)
            gg_ref[at, cols(j)] = (first * a_ref[at, cols(j)].astype(F32) * (1.0 - sg)).astype(BF16)
            return carry

        lax.fori_loop(0, tiles, step, 0)

    for b in range(blocks - 1):
        back(b)

    @pl.when(me < owners)
    def _():
        rs_in[me] = red_s[part(me), :]
        peers(lambda peer: rs_copy(me, peer, peer).wait_recv())
        ag_src[...] = lax.fori_loop(
            1, n, lambda s, total: total + rs_in[s], rs_in[0]
        )
        peers(lambda peer: ag_copy(me, peer).start())
        ag_in[part(me), :] = ag_src[...]

    @pl.when(me < n - 1)
    def _():
        dc_copy.wait_recv()

        def widen(j, carry):
            d_s[j, pl.ds(rows, HALO), :] = dc_in[j].astype(F32)
            return carry

        lax.fori_loop(0, tiles, widen, 0)

    @pl.when(me == n - 1)
    def _():
        def clear(j, carry):
            d_s[j, pl.ds(rows, HALO), :] = jnp.zeros((HALO, LANES), F32)
            return carry

        lax.fori_loop(0, tiles, clear, 0)

    back(blocks - 1)

    peers(lambda peer: rs_copy(peer, me, peer).wait_send(), owners)

    @pl.when(me < n - 1)
    def _():
        glu_copy.wait_send()

    @pl.when(me > 0)
    def _():
        dc_copy.wait_send()

    for i in range(2 * blocks):
        stat_copy(i).wait_send()

    peers(lambda peer: ag_copy(peer, peer).wait_recv(), owners)

    def finish(j, carry):
        at = pl.multiple_of(j * group, SUB)
        tg_ref[:, cols(j)] = ag_in[pl.ds(at, width), :]
        gaing_ref[:, cols(j)] = ag_in[pl.ds(at + width, 1), :]
        shiftg_ref[:, cols(j)] = ag_in[pl.ds(at + width + 1, 1), :]
        return carry

    lax.fori_loop(0, tiles, finish, 0)

    @pl.when(me < owners)
    def _():
        peers(lambda peer: ag_copy(me, peer).wait_send())


def solution(mesh):
    n, ntp = mesh.shape["sp"], mesh.shape["tp"]

    def body(proj_a, proj_gate, taps, norm_gain, norm_shift, cotangent):
        rows, chans = proj_a.shape
        width = taps.shape[0]
        tiles, group, chunk, owners = plan(chans, width, n)
        blocks = rows // BLOCK
        vmem = pl.BlockSpec(memory_space=pltpu.VMEM)
        grads = pl.pallas_call(
            functools.partial(kernel, n, ntp, width, chans * ntp),
            out_shape=(
                jax.ShapeDtypeStruct((rows, chans), BF16),
                jax.ShapeDtypeStruct((rows, chans), BF16),
                jax.ShapeDtypeStruct((width, chans), F32),
                jax.ShapeDtypeStruct((1, chans), F32),
                jax.ShapeDtypeStruct((1, chans), F32),
            ),
            in_specs=[vmem] * 6,
            out_specs=(vmem,) * 5,
            scratch_shapes=[
                pltpu.VMEM((tiles, HALO + rows, LANES), F32),
                pltpu.VMEM((tiles, rows, LANES), F32),
                pltpu.VMEM((tiles, rows, LANES), F32),
                pltpu.VMEM((tiles, rows + HALO, LANES), F32),
                pltpu.VMEM((tiles, -(-width // SUB) * SUB, LANES), F32),
                pltpu.VMEM((tiles, 3 * SUB, LANES), F32),
                pltpu.VMEM((tiles, HALO, LANES), BF16),
                pltpu.VMEM((tiles, HALO, LANES), BF16),
                pltpu.VMEM((tiles, HALO, LANES), BF16),
                pltpu.VMEM((tiles, HALO, LANES), BF16),
                pltpu.VMEM((2 * blocks, BLOCK, LANES), F32),
                pltpu.VMEM((2 * blocks, BLOCK, LANES), F32),
                pltpu.VMEM((3, rows, LANES), F32),
                pltpu.VMEM((owners * chunk, LANES), F32),
                pltpu.VMEM((n, chunk, LANES), F32),
                pltpu.VMEM((chunk, LANES), F32),
                pltpu.VMEM((owners * chunk, LANES), F32),
                pltpu.SemaphoreType.DMA((2,)),
                pltpu.SemaphoreType.DMA((2,)),
                pltpu.SemaphoreType.DMA((2 * blocks,)),
                pltpu.SemaphoreType.DMA((2 * blocks,)),
                pltpu.SemaphoreType.DMA((n,)),
                pltpu.SemaphoreType.DMA((n,)),
                pltpu.SemaphoreType.DMA((n,)),
                pltpu.SemaphoreType.DMA((n,)),
            ],
            compiler_params=pltpu.CompilerParams(collective_id=0, has_side_effects=True),
        )(
            proj_a, proj_gate, taps, norm_gain.reshape(1, chans),
            norm_shift.reshape(1, chans), cotangent,
        )
        a_grad, gate_grad, taps_grad, gain_grad, shift_grad = grads
        return (
            a_grad, gate_grad, taps_grad, gain_grad.reshape(chans), shift_grad.reshape(chans)
        )

    placed = (P("sp", "tp"), P("sp", "tp"), P(None, "tp"), P("tp"), P("tp"), P("sp", "tp"))
    return jax.shard_map(
        body,
        mesh=mesh,
        in_specs=placed,
        out_specs=(P("sp", "tp"), P("sp", "tp"), P(None, "tp"), P("tp"), P("tp")),
        check_vma=False,
    )
```

time: 186 us -> 49.2 us (0.26)
  the two profiles are of different devices: /device:TPU:0 before, /device:TPU:24 now
where the time goes in v1:
time: 49.2 us; the launch traced here: 48.9 us
  Pallas kernels  40.4 us (82%)
  local copies, waits for them, and re-layouts  6.59 us (13%)
  other arithmetic  1.24 us (3%)
  between operations  0.66 us (1%)
    pallas_call x1, Pallas kernels, body(): pl.pallas_call(functools.partial(kernel, n, ntp, width, chans * ntp), out...  40.4 us
    unnamed x13, local copies, waits for them, and re-layouts  4.69 us
    reshape x1, local copies, waits for them, and re-layouts, body(): norm_gain.reshape(1, chans)  1.3 us
    pallas_call x2, other arithmetic, body(): pl.pallas_call(functools.partial(kernel, n, ntp, width, chans * ntp), out...  1.24 us

profile of v1, /device:TPU:24, one launch (start us, length us, event | category | flops | bytes accessed | tf_op | source)
XLA Modules:
  0.0 48.9 jit_solution(14609045519192858721)
XLA Ops:
  0.6 0.0 copy-start.2
  0.6 1.3 %reshape.22.gain_ref = f32[1,1536]{1,0:T(1,128)} reshape(f32[1536]{0:T(1024)} %param.9) | data formatting | bytes 12288 | tf_op jit(solution)/shard_map/reshape | solution.py:402
  1.9 0.0 copy-done.2
  1.9 0.6 %reshape.23.shift_ref = f32[1,1536]{1,0:T(1,128)} reshape(f32[1536]{0:T(1024)S(1)} %copy-done.2) | data formatting | bytes 12288 | tf_op jit(solution)/shard_map/reshape | solution.py:403
  2.5 40.4 %shard_map.101 = (bf16[256,1536]{1,0:T(8,128)(2,1)}, bf16[256,1536]{1,0:T(8,128)(2,1)}, f32[31,1536]{1,0:T(8,128)}, f32[1,1536]{1,0:T(1,128)}, f32[1,1536]{1,0:T(1,128)}) custom-call(bf16[256,1536]{1,0:T(8,128)(2,1)} %a_ref.1, bf16[256,1536]{1,0:T(8,128)(2,1)} %g_ref.1, bf16[31,1536]{1,0:T(8,128)(2,1)} %taps_ref.1, f32[1,1536]{1,0:T(1,128)} %reshape.22.gain_ref, ...), custom_call_target="tpu_custom_call" | custom-call | tf_op jit(solution)/shard_map/pallas_call | solution.py:362
  42.9 0.0 copy-start.4
  42.9 0.7 %copy-done.4 = f32[1,1536]{1,0:T(1,128)S(1)} copy-done((f32[1,1536]{1,0:T(1,128)S(1)}, f32[1,1536]{1,0:T(1,128)}, u32[]{:S(2)}) %copy-start.4) | copy-done | bytes 6168
  43.6 0.0 copy-start.3
  43.6 0.6 %reduce = f32[1536]{0:T(1024)} reduce(f32[1,1536]{1,0:T(1,128)S(1)} %copy-done.4, f32[]{:T(128)} %constant), dimensions={0}, to_apply=%get-tuple-element.13.reduce_sub_computation | reduce | bytes 12292 | tf_op jit(solution)/shard_map/pallas_call | solution.py:362
  44.2 0.1 copy-done.3
  44.3 0.6 %reduce.1 = f32[1536]{0:T(1024)} reduce(f32[1,1536]{1,0:T(1,128)S(1)} %copy-done.3, f32[]{:T(128)} %constant), dimensions={0}, to_apply=%get-tuple-element.14.reduce_sub_computation | reduce | bytes 12292 | tf_op jit(solution)/shard_map/pallas_call | solution.py:362
  44.9 0.0 copy-start
  44.9 2.1 %copy.14 = bf16[256,1536]{1,0:T(8,128)(2,1)} copy(bf16[256,1536]{1,0:T(8,128)(2,1)} %get-tuple-element.20) | data formatting | bytes 1572864
  47.1 0.0 copy-done
  47.1 0.0 copy-start.1
  47.1 0.9 %copy.15 = bf16[256,1536]{1,0:T(8,128)(2,1)} copy(bf16[256,1536]{1,0:T(8,128)(2,1)S(1)} %copy-done) | data formatting | bytes 1572864
  48.0 0.2 copy-done.1
  48.2 0.7 %copy.16 = f32[31,1536]{1,0:T(8,128)} copy(f32[31,1536]{1,0:T(8,128)S(1)} %copy-done.1) | data formatting | bytes 380928
Async XLA Ops:
  0.6 1.3 %copy-start.2 = (f32[1536]{0:T(1024)S(1)}, f32[1536]{0:T(1024)}, u32[]{:S(2)}) copy-start(f32[1536]{0:T(1024)} %param.10) | copy-start | bytes 18436
  42.9 0.7 %copy-start.4 = (f32[1,1536]{1,0:T(1,128)S(1)}, f32[1,1536]{1,0:T(1,128)}, u32[]{:S(2)}) copy-start(f32[1,1536]{1,0:T(1,128)} %get-tuple-element.13) | copy-start | bytes 18436
  43.6 0.7 %copy-start.3 = (f32[1,1536]{1,0:T(1,128)S(1)}, f32[1,1536]{1,0:T(1,128)}, u32[]{:S(2)}) copy-start(f32[1,1536]{1,0:T(1,128)} %get-tuple-element.14) | copy-start | bytes 18436
  44.9 2.1 %copy-start = (bf16[256,1536]{1,0:T(8,128)(2,1)S(1)}, bf16[256,1536]{1,0:T(8,128)(2,1)}, u32[]{:S(2)}) copy-start(bf16[256,1536]{1,0:T(8,128)(2,1)} %get-tuple-element.21) | copy-start | bytes 2359300
  47.1 1.1 %copy-start.1 = (f32[31,1536]{1,0:T(8,128)S(1)}, f32[31,1536]{1,0:T(8,128)}, u32[]{:S(2)}) copy-start(f32[31,1536]{1,0:T(8,128)} %get-tuple-element.22) | copy-start | bytes 571396

commit v2 on v1

v2 whole, which is shorter than its diff:
```python
import functools

import jax
import jax.numpy as jnp
from jax import lax
from jax.experimental import pallas as pl
from jax.experimental.pallas import tpu as pltpu
from jax.sharding import PartitionSpec as P

EPS = 1e-05
LANES = 128
SUB = 8
BLOCK = 64
HALO = 32
F32 = jnp.float32
BF16 = jnp.bfloat16


PACK = 16


def plan(chans, width, n):
    tiles = chans // LANES
    rounds = 2 if tiles % 2 == 0 else 1
    group = -(-(width + 2) // SUB) * SUB
    total = tiles // rounds * group
    chunk = -(-total // (n * PACK)) * PACK
    owners = -(-total // chunk)
    return tiles, rounds, group, chunk, owners


def kernel(
    n, ntp, width, full,
    a_hbm, g_hbm, taps_hbm, gain_ref, shift_ref, cot_hbm,
    ag_ref, gg_ref, sums_ref,
    a_ref, g_ref, cot_ref, taps_ref, x_s, conv_s, dn_s, d_s, taps_s, par_s,
    glu_out, glu_in, dc_out, dc_in,
    st_out, st_in, stat_s,
    red_f, red_s, rs_in, ag_src, ag_in, in_sem,
    halo_send, halo_recv, st_send, st_recv,
    rs_send, rs_recv, ag_send, ag_recv,
):
    rows, chans = a_hbm.shape
    edge = width - 1
    lead = HALO - edge
    tiles, rounds, group, chunk, owners = plan(chans, width, n)
    part_tiles = tiles // rounds
    blocks = rows // BLOCK
    tail, body = pl.ds(rows - HALO, HALO), pl.ds(0, rows - HALO)
    loads = [
        pltpu.make_async_copy(src, dst, in_sem.at[i])
        for i, (src, dst) in enumerate((
            (g_hbm.at[tail, :], g_ref.at[tail, :]),
            (a_hbm.at[tail, :], a_ref.at[tail, :]),
            (g_hbm.at[body, :], g_ref.at[body, :]),
            (a_hbm.at[body, :], a_ref.at[body, :]),
            (taps_hbm, taps_ref),
            (cot_hbm, cot_ref),
        ))
    ]
    for load in loads:
        load.start()
    me = lax.axis_index("sp")
    core = lax.axis_index("tp")
    other = 1 - core

    barrier = pltpu.get_barrier_semaphore()

    def greet(step, carry):
        pl.semaphore_signal(barrier, inc=1, device_id={"sp": lax.rem(me + step, n)})
        return carry

    lax.fori_loop(1, n, greet, 0)
    pl.semaphore_signal(barrier, inc=1, device_id={"tp": other})

    def cols(j):
        return pl.ds(pl.multiple_of(j * LANES, LANES), LANES)

    def gate_tile(j, base, count):
        a = a_ref[pl.ds(base, count), cols(j)].astype(F32)
        g = g_ref[pl.ds(base, count), cols(j)].astype(F32)
        return (a * jax.nn.sigmoid(g)).astype(BF16)

    def last_rows(j, carry):
        glu_out[j] = gate_tile(j, rows - HALO, HALO)
        return carry

    loads[0].wait()
    loads[1].wait()
    lax.fori_loop(0, tiles, last_rows, 0)

    glu_copy = pltpu.make_async_remote_copy(
        src_ref=glu_out, dst_ref=glu_in, send_sem=halo_send.at[0], recv_sem=halo_recv.at[0],
        device_id={"sp": lax.rem(me + 1, n)},
    )
    dc_copy = pltpu.make_async_remote_copy(
        src_ref=dc_out, dst_ref=dc_in, send_sem=halo_send.at[1], recv_sem=halo_recv.at[1],
        device_id={"sp": lax.rem(me + n - 1, n)},
    )

    def prepare(j, carry):
        taps_s[j, pl.ds(0, width), :] = taps_ref[:, cols(j)].astype(F32)
        par_s[j, 0:1, :] = gain_ref[cols(j)].reshape(1, LANES)
        par_s[j, 1:2, :] = shift_ref[cols(j)].reshape(1, LANES)
        par_s[j, pl.ds(SUB, 2 * SUB), :] = jnp.zeros((2 * SUB, LANES), F32)
        for b in range(blocks):
            x_s[j, pl.ds(HALO + b * BLOCK, BLOCK), :] = gate_tile(j, b * BLOCK, BLOCK).astype(F32)
        return carry

    for load in loads[2:5]:
        load.wait()
    pl.semaphore_wait(barrier, n)

    @pl.when(me < n - 1)
    def _():
        glu_copy.start()

    lax.fori_loop(0, tiles, prepare, 0)

    lane = lax.broadcasted_iota(jnp.int32, (BLOCK, LANES), 1)

    def stat_copy(i):
        return pltpu.make_async_remote_copy(
            src_ref=st_out.at[i], dst_ref=st_in.at[i], send_sem=st_send.at[i],
            recv_sem=st_recv.at[i], device_id={"tp": other},
        )

    def send_stats(i, first, second):
        first = jnp.sum(first, axis=1, keepdims=True)
        second = jnp.sum(second, axis=1, keepdims=True)
        st_out[i] = jnp.where(lane < LANES // 2, first, second)
        stat_copy(i).start()

    def both_stats(i):
        stat_copy(i).wait_recv()
        both = (st_out[i] + st_in[i]) * (1.0 / full)
        first = jnp.broadcast_to(both[:, 0:1], (BLOCK, LANES))
        second = jnp.broadcast_to(both[:, LANES // 2 : LANES // 2 + 1], (BLOCK, LANES))
        return first, second

    zero = jnp.zeros((BLOCK, LANES), F32)

    def convolve(b):
        base = b * BLOCK

        def step(j, carry):
            first, second = carry
            acc = zero
            for k in range(width):
                acc = acc + taps_s[j, k : k + 1, :] * x_s[j, pl.ds(base + lead + k, BLOCK), :]
            conv_s[j, pl.ds(base, BLOCK), :] = acc
            return first + acc, second + acc * acc

        first, second = lax.fori_loop(0, tiles, step, (zero, zero))
        send_stats(b, first, second)

    def fold(x):
        return jnp.sum(x.reshape(x.shape[0] // SUB, SUB, LANES), axis=0)

    def normalise(b):
        base = b * BLOCK
        mean, square = both_stats(b)
        rstd = lax.rsqrt(jnp.maximum(square - mean * mean, 0.0) + EPS)
        stat_s[0, pl.ds(base, BLOCK), :] = rstd

        def step(j, carry):
            first, second = carry
            at = pl.ds(base, BLOCK)
            gain = par_s[j, 0:1, :]
            normed = (conv_s[j, at, :] - mean) * rstd
            pre = normed * gain + par_s[j, 1:2, :]
            sig = jax.nn.sigmoid(pre)
            dpre = cot_ref[at, cols(j)].astype(F32) * sig * (1.0 + pre * (1.0 - sig))
            par_s[j, pl.ds(SUB, SUB), :] += fold(dpre * normed)
            par_s[j, pl.ds(2 * SUB, SUB), :] += fold(dpre)
            dn = dpre * gain
            conv_s[j, at, :] = normed
            dn_s[j, at, :] = dn
            return first + dn, second + dn * normed

        first, second = lax.fori_loop(0, tiles, step, (zero, zero))
        send_stats(blocks + b, first, second)

    def take_stats(b):
        first, second = both_stats(blocks + b)
        at = pl.ds(b * BLOCK, BLOCK)
        stat_s[1, at, :] = first
        stat_s[2, at, :] = second

    def dconv_at(j, at):
        return stat_s[0, at, :] * (
            dn_s[j, at, :] - stat_s[1, at, :] - conv_s[j, at, :] * stat_s[2, at, :]
        )

    for b in range(1, blocks):
        convolve(b)
    loads[5].wait()
    for b in range(1, blocks):
        normalise(b)

    @pl.when(me > 0)
    def _():
        glu_copy.wait_recv()

        def widen(j, carry):
            x_s[j, pl.ds(0, HALO), :] = glu_in[j].astype(F32)
            return carry

        lax.fori_loop(0, tiles, widen, 0)

    @pl.when(me == 0)
    def _():
        def clear(j, carry):
            x_s[j, pl.ds(0, HALO), :] = jnp.zeros((HALO, LANES), F32)
            return carry

        lax.fori_loop(0, tiles, clear, 0)

    convolve(0)
    for b in range(1, blocks):
        take_stats(b)
    normalise(0)
    take_stats(0)

    def head(j, carry):
        dc_out[j] = dconv_at(j, pl.ds(0, HALO)).astype(BF16)
        return carry

    lax.fori_loop(0, tiles, head, 0)

    @pl.when(me > 0)
    def _():
        dc_copy.start()

    spare = owners * chunk - part_tiles * group

    def taps_round(h):
        def step(i, carry):
            j = h * part_tiles + i
            d = dconv_at(j, pl.ds(0, rows))
            d_s[j, pl.ds(0, rows), :] = d
            at = pl.multiple_of(i * group, SUB)
            for k in range(width):
                prod = d * x_s[j, pl.ds(lead + k, rows), :]
                red_f[pl.ds(at + k, 1), :] = jnp.sum(prod, axis=0, keepdims=True)
            for k in range(2):
                red_f[pl.ds(at + width + k, 1), :] = jnp.sum(
                    par_s[j, pl.ds(SUB + k * SUB, SUB), :], axis=0, keepdims=True
                )
            for k in range(width + 2, group):
                red_f[pl.ds(at + k, 1), :] = jnp.zeros((1, LANES), F32)
            return carry

        lax.fori_loop(0, part_tiles, step, 0)
        if spare:
            red_f[pl.ds(part_tiles * group, spare), :] = jnp.zeros((spare, LANES), F32)
        red_s[h] = red_f[...].astype(BF16)

    def part(owner):
        return pl.ds(pl.multiple_of(owner * chunk, PACK), chunk)

    def rs_copy(h, owner, source, to):
        return pltpu.make_async_remote_copy(
            src_ref=red_s.at[h, part(owner), :], dst_ref=rs_in.at[h, source],
            send_sem=rs_send.at[h * n + owner], recv_sem=rs_recv.at[h * n + source],
            device_id={"sp": to},
        )

    def ag_copy(h, owner, to):
        return pltpu.make_async_remote_copy(
            src_ref=ag_src.at[h], dst_ref=ag_in.at[h, part(owner), :],
            send_sem=ag_send.at[h * n + to], recv_sem=ag_recv.at[h * n + owner],
            device_id={"sp": to},
        )

    def peers(run, limit=n):
        def step(d, carry):
            peer = lax.rem(me + d, n)
            if limit == n:
                run(peer)
            else:
                pl.when(peer < limit)(lambda: run(peer))
            return carry

        lax.fori_loop(1, n, step, 0)

    def scatter(h):
        peers(lambda peer: rs_copy(h, peer, me, peer).start(), owners)

    def gather(h):
        @pl.when(me < owners)
        def _():
            rs_in[h, me] = red_s[h, part(me), :]
            peers(lambda peer: rs_copy(h, me, peer, peer).wait_recv())
            ag_src[h] = lax.fori_loop(
                1, n, lambda s, total: total + rs_in[h, s].astype(F32), rs_in[h, 0].astype(F32)
            ).astype(BF16)
            peers(lambda peer: ag_copy(h, me, peer).start())
            ag_in[h, part(me), :] = ag_src[h]

    for h in range(rounds):
        taps_round(h)
        scatter(h)

    def back(b):
        base = b * BLOCK

        def step(j, carry):
            acc = zero
            for k in range(width):
                acc = acc + taps_s[j, edge - k : edge - k + 1, :] * d_s[j, pl.ds(base + k, BLOCK), :]
            at = pl.ds(base, BLOCK)
            sg = jax.nn.sigmoid(g_ref[at, cols(j)].astype(F32))
            first = acc * sg
            ag_ref[at, cols(j)] = first.astype(BF16)
            gg_ref[at, cols(j)] = (first * a_ref[at, cols(j)].astype(F32) * (1.0 - sg)).astype(BF16)
            return carry

        lax.fori_loop(0, tiles, step, 0)

    back(0)
    for h in range(rounds - 1):
        gather(h)
    for b in range(1, blocks - 1):
        back(b)

    @pl.when(me < n - 1)
    def _():
        dc_copy.wait_recv()

        def widen(j, carry):
            d_s[j, pl.ds(rows, HALO), :] = dc_in[j].astype(F32)
            return carry

        lax.fori_loop(0, tiles, widen, 0)

    @pl.when(me == n - 1)
    def _():
        def clear(j, carry):
            d_s[j, pl.ds(rows, HALO), :] = jnp.zeros((HALO, LANES), F32)
            return carry

        lax.fori_loop(0, tiles, clear, 0)

    back(blocks - 1)
    gather(rounds - 1)

    for h in range(rounds):
        peers(lambda peer: rs_copy(h, peer, me, peer).wait_send(), owners)

    @pl.when(me < n - 1)
    def _():
        glu_copy.wait_send()

    @pl.when(me > 0)
    def _():
        dc_copy.wait_send()

    for i in range(2 * blocks):
        stat_copy(i).wait_send()

    for h in range(rounds):
        peers(lambda peer: ag_copy(h, peer, peer).wait_recv(), owners)
        sums_ref[h] = ag_in[h].astype(F32)

    @pl.when(me < owners)
    def _():
        for h in range(rounds):
            peers(lambda peer: ag_copy(h, me, peer).wait_send())


def finish(width, part_tiles, group, ag_ref, gg_ref, sums_ref, ag_out, gg_out, tg_ref, gaing_ref, shiftg_ref, sems):
    first = pltpu.make_async_copy(ag_ref, ag_out, sems.at[0])
    second = pltpu.make_async_copy(gg_ref, gg_out, sems.at[1])
    first.start()
    second.start()
    for h in range(sums_ref.shape[0]):
        for i in range(part_tiles):
            at = pl.ds((h * part_tiles + i) * LANES, LANES)
            tg_ref[:, at] = sums_ref[h, pl.ds(i * group, width), :]
            gaing_ref[at] = sums_ref[h, i * group + width, :]
            shiftg_ref[at] = sums_ref[h, i * group + width + 1, :]
    first.wait()
    second.wait()


def solution(mesh):
    n, ntp = mesh.shape["sp"], mesh.shape["tp"]

    def body(proj_a, proj_gate, taps, norm_gain, norm_shift, cotangent):
        rows, chans = proj_a.shape
        width = taps.shape[0]
        tiles, rounds, group, chunk, owners = plan(chans, width, n)
        blocks = rows // BLOCK
        vmem = pl.BlockSpec(memory_space=pltpu.VMEM)
        hbm = pl.BlockSpec(memory_space=pltpu.HBM)
        wide = jax.ShapeDtypeStruct((rows, chans), BF16)
        a_grad, gate_grad, sums = pl.pallas_call(
            functools.partial(kernel, n, ntp, width, chans * ntp),
            out_shape=(wide, wide, jax.ShapeDtypeStruct((rounds, owners * chunk, LANES), F32)),
            in_specs=[hbm, hbm, hbm, vmem, vmem, hbm],
            out_specs=(vmem,) * 3,
            scratch_shapes=[
                pltpu.VMEM((rows, chans), BF16),
                pltpu.VMEM((rows, chans), BF16),
                pltpu.VMEM((rows, chans), BF16),
                pltpu.VMEM((width, chans), BF16),
                pltpu.VMEM((tiles, HALO + rows, LANES), F32),
                pltpu.VMEM((tiles, rows, LANES), F32),
                pltpu.VMEM((tiles, rows, LANES), F32),
                pltpu.VMEM((tiles, rows + HALO, LANES), F32),
                pltpu.VMEM((tiles, -(-width // SUB) * SUB, LANES), F32),
                pltpu.VMEM((tiles, 3 * SUB, LANES), F32),
                pltpu.VMEM((tiles, HALO, LANES), BF16),
                pltpu.VMEM((tiles, HALO, LANES), BF16),
                pltpu.VMEM((tiles, HALO, LANES), BF16),
                pltpu.VMEM((tiles, HALO, LANES), BF16),
                pltpu.VMEM((2 * blocks, BLOCK, LANES), F32),
                pltpu.VMEM((2 * blocks, BLOCK, LANES), F32),
                pltpu.VMEM((3, rows, LANES), F32),
                pltpu.VMEM((owners * chunk, LANES), F32),
                pltpu.VMEM((rounds, owners * chunk, LANES), BF16),
                pltpu.VMEM((rounds, n, chunk, LANES), BF16),
                pltpu.VMEM((rounds, chunk, LANES), BF16),
                pltpu.VMEM((rounds, owners * chunk, LANES), BF16),
                pltpu.SemaphoreType.DMA((6,)),
                pltpu.SemaphoreType.DMA((2,)),
                pltpu.SemaphoreType.DMA((2,)),
                pltpu.SemaphoreType.DMA((2 * blocks,)),
                pltpu.SemaphoreType.DMA((2 * blocks,)),
                pltpu.SemaphoreType.DMA((rounds * n,)),
                pltpu.SemaphoreType.DMA((rounds * n,)),
                pltpu.SemaphoreType.DMA((rounds * n,)),
                pltpu.SemaphoreType.DMA((rounds * n,)),
            ],
            compiler_params=pltpu.CompilerParams(
                collective_id=0, has_side_effects=True, vmem_limit_bytes=32 * 1024 * 1024
            ),
        )(proj_a, proj_gate, taps, norm_gain, norm_shift, cotangent)
        vector = jax.ShapeDtypeStruct((chans,), F32)
        return pl.pallas_call(
            functools.partial(finish, width, tiles // rounds, group),
            out_shape=(wide, wide, jax.ShapeDtypeStruct((width, chans), F32), vector, vector),
            in_specs=[vmem] * 3,
            out_specs=(hbm, hbm, vmem, vmem, vmem),
            scratch_shapes=[pltpu.SemaphoreType.DMA((2,))],
            compiler_params=pltpu.CompilerParams(vmem_limit_bytes=16 * 1024 * 1024),
        )(a_grad, gate_grad, sums)

    placed = (P("sp", "tp"), P("sp", "tp"), P(None, "tp"), P("tp"), P("tp"), P("sp", "tp"))
    return jax.shard_map(
        body,
        mesh=mesh,
        in_specs=placed,
        out_specs=(P("sp", "tp"), P("sp", "tp"), P(None, "tp"), P("tp"), P("tp")),
        check_vma=False,
    )
```

time: 49.2 us -> 41.5 us (0.84)
  the two profiles are of different devices: /device:TPU:24 before, /device:TPU:0 now
where the time goes in v2:
time: 41.5 us; the launch traced here: 41.1 us
  Pallas kernels  34.8 us (84%)
  local copies, waits for them, and re-layouts  5.68 us (14%)
  between operations  0.65 us (2%)
    pallas_call x1, Pallas kernels, body(): pl.pallas_call(functools.partial(kernel, n, ntp, width, chans * ntp), out...  32.9 us
    unnamed x12, local copies, waits for them, and re-layouts  5.68 us
    pallas_call x1, Pallas kernels, body(): pl.pallas_call(functools.partial(finish, width, tiles // rounds, group),...  1.84 us

profile of v2, /device:TPU:0, one launch (start us, length us, event | category | flops | bytes accessed | tf_op | source)
XLA Modules:
  0.0 41.1 jit_solution(12650901455847624784)
XLA Ops:
  0.6 0.0 copy-start
  0.6 1.1 %copy-done = bf16[256,1536]{1,0:T(8,128)(2,1)S(1)} copy-done((bf16[256,1536]{1,0:T(8,128)(2,1)S(1)}, bf16[256,1536]{1,0:T(8,128)(2,1)}, u32[]{:S(2)}) %copy-start) | copy-done | bytes 786456
  1.8 0.0 copy-start.1
  1.8 1.1 %copy-done.1 = bf16[256,1536]{1,0:T(8,128)(2,1)S(1)} copy-done((bf16[256,1536]{1,0:T(8,128)(2,1)S(1)}, bf16[256,1536]{1,0:T(8,128)(2,1)}, u32[]{:S(2)}) %copy-start.1) | copy-done | bytes 786456
  2.9 0.0 copy-start.2
  2.9 1.1 %copy-done.2 = bf16[256,1536]{1,0:T(8,128)(2,1)S(1)} copy-done((bf16[256,1536]{1,0:T(8,128)(2,1)S(1)}, bf16[256,1536]{1,0:T(8,128)(2,1)}, u32[]{:S(2)}) %copy-start.2) | copy-done | bytes 786456
  4.0 0.0 copy-start.3
  4.0 0.9 %copy-done.3 = bf16[31,1536]{1,0:T(8,128)(2,1)S(1)} copy-done((bf16[31,1536]{1,0:T(8,128)(2,1)S(1)}, bf16[31,1536]{1,0:T(8,128)(2,1)}, u32[]{:S(2)}) %copy-start.3) | copy-done | bytes 95256
  4.9 0.0 copy-start.4
  4.9 0.7 %copy-done.4 = f32[1536]{0:T(1024)S(1)} copy-done((f32[1536]{0:T(1024)S(1)}, f32[1536]{0:T(1024)}, u32[]{:S(2)}) %copy-start.4) | copy-done | bytes 6168
  5.6 0.0 copy-start.5
  5.6 0.7 %copy-done.5 = f32[1536]{0:T(1024)S(1)} copy-done((f32[1536]{0:T(1024)S(1)}, f32[1536]{0:T(1024)}, u32[]{:S(2)}) %copy-start.5) | copy-done | bytes 6168
  6.3 32.9 %shard_map.101 = (bf16[256,1536]{1,0:T(8,128)(2,1)S(1)}, bf16[256,1536]{1,0:T(8,128)(2,1)S(1)}, f32[2,240,128]{2,1,0:T(8,128)S(1)}) custom-call(bf16[256,1536]{1,0:T(8,128)(2,1)S(1)} %copy-done, bf16[256,1536]{1,0:T(8,128)(2,1)S(1)} %copy-done.1, bf16[31,1536]{1,0:T(8,128)(2,1)S(1)} %copy-done.3, f32[1536]{0:T(1024)S(1)} %copy-done.4, f32[1536]{0:T(1024)S(1)} %copy-done.5, ...), custom_call_target="tpu_custom_call" | custom-call | tf_op jit(solution)/shard_map/pallas_call | solution.py:398
  39.3 1.8 %shard_map.102 = (bf16[256,1536]{1,0:T(8,128)(2,1)}, bf16[256,1536]{1,0:T(8,128)(2,1)}, f32[31,1536]{1,0:T(8,128)}, f32[1536]{0:T(1024)}, f32[1536]{0:T(1024)}) custom-call(bf16[256,1536]{1,0:T(8,128)(2,1)S(1)} %get-tuple-element.8.ag_ref, bf16[256,1536]{1,0:T(8,128)(2,1)S(1)} %get-tuple-element.9.gg_ref, f32[2,240,128]{2,1,0:T(8,128)S(1)} %get-tuple-element.10.sums_ref), custom_call_target="tpu_custom_call" | custom-call | tf_op jit(solution)/shard_map/pallas_call | solution.py:441
Async XLA Ops:
  0.6 1.1 %copy-start = (bf16[256,1536]{1,0:T(8,128)(2,1)S(1)}, bf16[256,1536]{1,0:T(8,128)(2,1)}, u32[]{:S(2)}) copy-start(bf16[256,1536]{1,0:T(8,128)(2,1)} %a_hbm.1) | copy-start | bytes 2359300
  1.8 1.1 %copy-start.1 = (bf16[256,1536]{1,0:T(8,128)(2,1)S(1)}, bf16[256,1536]{1,0:T(8,128)(2,1)}, u32[]{:S(2)}) copy-start(bf16[256,1536]{1,0:T(8,128)(2,1)} %g_hbm.1) | copy-start | bytes 2359300
  2.9 1.1 %copy-start.2 = (bf16[256,1536]{1,0:T(8,128)(2,1)S(1)}, bf16[256,1536]{1,0:T(8,128)(2,1)}, u32[]{:S(2)}) copy-start(bf16[256,1536]{1,0:T(8,128)(2,1)} %cot_hbm.1) | copy-start | bytes 2359300
  4.0 0.9 %copy-start.3 = (bf16[31,1536]{1,0:T(8,128)(2,1)S(1)}, bf16[31,1536]{1,0:T(8,128)(2,1)}, u32[]{:S(2)}) copy-start(bf16[31,1536]{1,0:T(8,128)(2,1)} %taps_hbm.1) | copy-start | bytes 285700
  4.9 0.7 %copy-start.4 = (f32[1536]{0:T(1024)S(1)}, f32[1536]{0:T(1024)}, u32[]{:S(2)}) copy-start(f32[1536]{0:T(1024)} %gain_ref.1) | copy-start | bytes 18436
  5.6 0.7 %copy-start.5 = (f32[1536]{0:T(1024)S(1)}, f32[1536]{0:T(1024)}, u32[]{:S(2)}) copy-start(f32[1536]{0:T(1024)} %shift_ref.1) | copy-start | bytes 18436

commit v3 on v2

--- a/solution.py
+++ b/solution.py
@@ -436,7 +436,10 @@
             compiler_params=pltpu.CompilerParams(
                 collective_id=0, has_side_effects=True, vmem_limit_bytes=32 * 1024 * 1024
             ),
-        )(proj_a, proj_gate, taps, norm_gain, norm_shift, cotangent)
+        )(*(
+            pltpu.with_memory_space_constraint(x, pltpu.HBM)
+            for x in (proj_a, proj_gate, taps, norm_gain, norm_shift, cotangent)
+        ))
         vector = jax.ShapeDtypeStruct((chans,), F32)
         return pl.pallas_call(
             functools.partial(finish, width, tiles // rounds, group),

time: 41.5 us -> 35.5 us (0.86)
  local copies, waits for them, and re-layouts: 5.68 us -> 0 us
    unnamed x12 -> x0, local copies, waits for them, and re-layouts: 5.68 us -> none
where the time goes in v3:
time: 35.5 us; the launch traced here: 35.2 us
  Pallas kernels  34.6 us (97%)
  between operations  0.64 us (2%)
    pallas_call x1, Pallas kernels, body(): pl.pallas_call(functools.partial(kernel, n, ntp, width, chans * ntp), out...  32.7 us
    pallas_call x1, Pallas kernels, body(): pl.pallas_call(functools.partial(finish, width, tiles // rounds, group),...  1.84 us

profile of v3, /device:TPU:0, one launch (start us, length us, event | category | flops | bytes accessed | tf_op | source)
XLA Modules:
  0.0 35.2 jit_solution(8808627965042767567)
XLA Ops:
  0.6 32.7 %shard_map.101 = (bf16[256,1536]{1,0:T(8,128)(2,1)S(1)}, bf16[256,1536]{1,0:T(8,128)(2,1)S(1)}, f32[2,240,128]{2,1,0:T(8,128)S(1)}) custom-call(bf16[256,1536]{1,0:T(8,128)(2,1)} %a_hbm.1, bf16[256,1536]{1,0:T(8,128)(2,1)} %g_hbm.1, bf16[31,1536]{1,0:T(8,128)(2,1)} %taps_hbm.1, f32[1536]{0:T(1024)} %gain_ref.1, f32[1536]{0:T(1024)} %shift_ref.1, ...), custom_call_target="tpu_custom_call" | custom-call | tf_op jit(solution)/shard_map/pallas_call | solution.py:398
  33.4 1.8 %shard_map.102 = (bf16[256,1536]{1,0:T(8,128)(2,1)}, bf16[256,1536]{1,0:T(8,128)(2,1)}, f32[31,1536]{1,0:T(8,128)}, f32[1536]{0:T(1024)}, f32[1536]{0:T(1024)}) custom-call(bf16[256,1536]{1,0:T(8,128)(2,1)S(1)} %get-tuple-element.8.ag_ref, bf16[256,1536]{1,0:T(8,128)(2,1)S(1)} %get-tuple-element.9.gg_ref, f32[2,240,128]{2,1,0:T(8,128)S(1)} %get-tuple-element.10.sums_ref), custom_call_target="tpu_custom_call" | custom-call | tf_op jit(solution)/shard_map/pallas_call | solution.py:444
